TPU v7x, 512 devices: a whole 4x8x8 slice. The times are simulated.
512 devices in a mesh: tp: 64 (over z, y), dp: 8 (over x, core).
Axes of the slice: x: 4, y: 8, z: 8, core: 2. Of those that a mesh axis runs over, the one named last changes fastest.
Arguments:
- hidden: bfloat16 [64, 4096], P(None, 'dp'), may hold values from -6 to 6
- norm_gain: float32 [2, 4096], P(None, 'dp'), may hold values from 0.1 to 1.9
- gate_weight: bfloat16 [2, 4096, 8192], P(None, 'dp', 'tp'), may hold values from -0.09375 to 0.09375
- inner_weight: bfloat16 [2, 4096, 8192], P(None, 'dp', 'tp'), may hold values from -0.09375 to 0.09375
- write_weight: bfloat16 [2, 4096, 2048], P(None, 'dp', 'tp'), may hold values from -0.09375 to 0.09375
- read_weight: bfloat16 [2, 4096, 2048], P(None, 'dp', 'tp'), may hold values from -0.09375 to 0.09375
- step_weight: bfloat16 [2, 4096, 128], P(None, 'dp'), may hold values from -0.09375 to 0.09375
- conv_inner: bfloat16 [2, 4, 8192], P(None, None, 'tp'), may hold values from -3 to 3
- conv_write: bfloat16 [2, 4, 2048], P(None, None, 'tp'), may hold values from -3 to 3
- conv_read: bfloat16 [2, 4, 2048], P(None, None, 'tp'), may hold values from -3 to 3
- step_bias: float32 [2, 128], P(None, 'tp'), may hold values from -4 to -1
- decay_log: float32 [2, 128], P(None, 'tp'), may hold values from -3 to 0.5
- skip_gain: float32 [2, 128], P(None, 'tp'), may hold values from 0.1 to 1.9
- group_gain: float32 [2, 8192], P(None, 'tp'), may hold values from 0.1 to 1.9
- out_weight: bfloat16 [2, 8192, 4096], P(None, 'tp', 'dp'), may hold values from -0.4 to 0.4
- state_inner: bfloat16 [2, 64, 3, 8192], P(None, 'dp', None, 'tp'), may hold values from -6 to 6
- state_write: bfloat16 [2, 64, 3, 2048], P(None, 'dp', None, 'tp'), may hold values from -6 to 6
- state_read: bfloat16 [2, 64, 3, 2048], P(None, 'dp', None, 'tp'), may hold values from -6 to 6
- recurrent: float32 [2, 64, 128, 64, 128], P(None, 'dp', 'tp'), may hold values from -1.2 to 1.2, as said below
Outputs:
- out_hidden: bfloat16 [64, 4096], P(None, 'dp')
- next_inner: bfloat16 [2, 64, 3, 8192], P(None, 'dp', None, 'tp')
- next_write: bfloat16 [2, 64, 3, 2048], P(None, 'dp', None, 'tp')
- next_read: bfloat16 [2, 64, 3, 2048], P(None, 'dp', None, 'tp')
- next_recurrent: float32 [2, 64, 128, 64, 128], P(None, 'dp', 'tp')
Inputs may be any that keep to these rules, and one draw needn't show every extreme that they name: recurrent states of order a tenth, with scales that differ between heads.
All inputs are finite; a program needn't handle non-finite values.
Results may differ from a plain program's by a relative error of at most 0.025.
Values may be sent and summed in bfloat16 or wider, within the bound.
No kernel may reach another device: no remote copies, remote signals or barrier semaphores. Data moves between devices by JAX's collectives and lax.ppermute only.
A program may use at most 64 MiB of HBM per device.

v0:
```python
import jax
import jax.numpy as jnp
from jax import lax
from jax.sharding import Mesh
from jax.sharding import PartitionSpec as P

D = 4096
HEADS = 128
GROUPS = 16
DP = ("dp_0", "dp_1")
TP = ("tp_0", "tp_1")
TP_DP = ("tp_0", "tp_1", "dp_0", "dp_1")
eps = 1e-06


def cut_along(shard, dim, size):
    before, after = (shard.shape[:dim], shard.shape[dim + 1 :])
    return jnp.moveaxis(shard.reshape(*before, size, -1, *after), dim, 0)


def summed_on_arrival(shard, axis, dim):
    size = lax.axis_size(axis)
    pieces = lax.all_to_all(cut_along(shard, dim, size), axis, 0, 0, tiled=True)
    return jnp.sum(pieces.astype(jnp.float32), axis=0)


def side_by_side(arrays, axis, dim, along):
    widths = [a.shape[along] for a in arrays]
    both = jnp.concatenate(arrays, axis=along)
    result = summed_on_arrival(both, axis, dim)
    return tuple(jnp.split(result, [sum(widths[:k]) for k in range(1, len(widths))], axis=along))


def gather_turned(arrays, axis, dims):
    turned = [jnp.moveaxis(a, dim, 0) for a, dim in zip(arrays, dims)]
    both = jnp.concatenate([t.reshape(len(t), -1) for t in turned], axis=1)
    result, at, gathered = (lax.all_gather(both, axis, axis=0, tiled=True), 0, [])
    for t, dim in zip(turned, dims):
        share = result[:, at : at + t[0].size].reshape(-1, *t.shape[1:])
        gathered.append(jnp.moveaxis(share, 0, dim))
        at += t[0].size
    return tuple(gathered)


def over_axes(shard, axes):
    for axis in axes:
        shard = lax.psum(shard, axis)
    return shard


def copy_for_each(shard, axis):
    size = lax.axis_size(axis)
    return lax.all_to_all(
        jnp.broadcast_to(shard[None], (size, *shard.shape)), axis, 0, 0, tiled=True
    )


def laid_out(pieces, dim):
    lengths = list(pieces.shape[1:])
    lengths[dim] *= pieces.shape[0]
    return jnp.moveaxis(pieces, 0, dim).reshape(lengths)


def collect(shard, axis, dim):
    pieces = copy_for_each(shard, axis)
    return laid_out(pieces, dim)


def summed_on_arrival_2(shard, axis, dim):
    pieces = cut_along(shard, dim, lax.axis_size(axis))
    arrived = lax.all_to_all(pieces, axis, split_axis=0, concat_axis=0, tiled=True)
    return arrived.sum(axis=0)


def taken_together(shard, axis):
    return copy_for_each(shard, axis).sum(axis=0)


def convolve(state, fresh_row, kernel):
    window = jnp.concatenate([state, fresh_row[:, None, :]], axis=1)
    summed = jnp.sum(window.astype(jnp.float32) * kernel.astype(jnp.float32)[None], axis=1)
    return (jax.nn.silu(summed), window[:, 1:])


def mixer_block(normed, number, weights):
    (
        gate_weight,
        inner_weight,
        write_weight,
        read_weight,
        step_weight,
        conv_inner,
        conv_write,
        conv_read,
        step_bias,
        decay_log,
        skip_gain,
        group_gain,
        out_weight,
        state_inner,
        state_write,
        state_read,
        recurrent,
    ) = weights

    def partial_of(weight):
        return jnp.dot(normed, weight[number], preferred_element_type=jnp.float32).astype(
            jnp.bfloat16
        )

    summed = side_by_side(
        (
            partial_of(gate_weight),
            partial_of(inner_weight),
            partial_of(write_weight),
            partial_of(read_weight),
            partial_of(step_weight),
        ),
        DP,
        0,
        1,
    )
    gate_raw, inner_raw, write_raw, read_raw, step_raw = [
        member.astype(jnp.bfloat16) for member in summed
    ]
    inner_act, next_inner = convolve(state_inner[number], inner_raw, conv_inner[number])
    write_act, next_write = convolve(state_write[number], write_raw, conv_write[number])
    read_act, next_read = convolve(state_read[number], read_raw, conv_read[number])
    write_all, read_all = gather_turned(
        (write_act.astype(jnp.bfloat16), read_act.astype(jnp.bfloat16)), TP, (1, 1)
    )
    heads_here = step_bias.shape[1]
    head_dim = recurrent.shape[3]
    state_dim = recurrent.shape[4]
    rows_here = inner_act.shape[0]
    first_head = lax.axis_index(TP) * heads_here
    group_index = first_head // (HEADS // GROUPS)
    write_grid = write_all.reshape(rows_here, state_dim, GROUPS)
    read_grid = read_all.reshape(rows_here, state_dim, GROUPS)
    write_vec = lax.dynamic_slice_in_dim(write_grid, group_index, 1, 2)[:, :, 0].astype(jnp.float32)
    read_vec = lax.dynamic_slice_in_dim(read_grid, group_index, 1, 2)[:, :, 0].astype(jnp.float32)
    step_own = lax.dynamic_slice_in_dim(step_raw, first_head, heads_here, 1)
    step_size = jax.nn.softplus(step_own.astype(jnp.float32) + step_bias[number][None, :])
    retain = jnp.exp(-step_size * jnp.exp(decay_log[number])[None, :])
    inner_heads = inner_act.reshape(rows_here, heads_here, head_dim)
    updated = (
        retain[:, :, None, None] * recurrent[number]
        + (step_size[:, :, None] * inner_heads)[:, :, :, None] * write_vec[:, None, None, :]
    )
    readout = jnp.einsum("bhpn,bn->bhp", updated, read_vec, precision=lax.Precision.HIGHEST)
    readout = readout + skip_gain[number][None, :, None] * inner_heads
    gated_out = readout.reshape(rows_here, heads_here * head_dim) * jax.nn.silu(
        gate_raw.astype(jnp.float32)
    )
    selector = (jnp.arange(GROUPS) == group_index).astype(jnp.float32)
    totals = over_axes(jnp.sum(gated_out * gated_out, axis=1)[:, None] * selector[None, :], TP)
    group_sum = jnp.sum(totals * selector[None, :], axis=1, keepdims=True)
    group_factor = lax.rsqrt(group_sum / (HEADS // GROUPS * head_dim) + eps)
    group_normed = (gated_out * group_factor * group_gain[number][None, :]).astype(jnp.bfloat16)
    branch = jnp.dot(
        collect(group_normed, DP, 0), out_weight[number], preferred_element_type=jnp.float32
    )
    return (branch, (next_inner, next_write, next_read, updated))


def columns_over(branch):
    return summed_on_arrival_2(branch, TP, 1)


def local(
    hidden,
    norm_gain,
    gate_weight,
    inner_weight,
    write_weight,
    read_weight,
    step_weight,
    conv_inner,
    conv_write,
    conv_read,
    step_bias,
    decay_log,
    skip_gain,
    group_gain,
    out_weight,
    state_inner,
    state_write,
    state_read,
    recurrent,
):
    weights = (
        gate_weight,
        inner_weight,
        write_weight,
        read_weight,
        step_weight,
        conv_inner,
        conv_write,
        conv_read,
        step_bias,
        decay_log,
        skip_gain,
        group_gain,
        out_weight,
        state_inner,
        state_write,
        state_read,
        recurrent,
    )
    wide_in = hidden.astype(jnp.float32)
    squares = taken_together(jnp.sum(wide_in * wide_in, axis=1, keepdims=True), DP)
    normed = (wide_in * lax.rsqrt(squares / D + eps) * norm_gain[0][None, :]).astype(jnp.bfloat16)
    branch, first_states = mixer_block(normed, 0, weights)
    slice_width = hidden.shape[1] // lax.axis_size(TP)
    offset = lax.axis_index(TP) * slice_width
    own_cols = lax.dynamic_slice_in_dim(wide_in, offset, slice_width, 1)
    middle = (own_cols + columns_over(branch)).astype(jnp.bfloat16).astype(jnp.float32)
    squares = over_axes(jnp.sum(middle * middle, axis=1, keepdims=True), TP_DP)
    gain_slice = lax.dynamic_slice_in_dim(norm_gain[1], offset, slice_width, 0)
    normed_part = (middle * lax.rsqrt(squares / D + eps) * gain_slice[None, :]).astype(jnp.bfloat16)
    normed = collect(normed_part, TP, 1)
    branch, second_states = mixer_block(normed, 1, weights)
    result = collect((middle + columns_over(branch)).astype(jnp.bfloat16), TP, 1)
    stacked = [jnp.stack([earlier, later]) for earlier, later in zip(first_states, second_states)]
    return (result, stacked[0], stacked[1], stacked[2], stacked[3])


def solution(mesh):
    finer = Mesh(mesh.devices.reshape(8, 8, 4, 2), ("tp_0", "tp_1", "dp_0", "dp_1"))
    placed = (
        P(None, DP),
        P(None, DP),
        P(None, DP, TP),
        P(None, DP, TP),
        P(None, DP, TP),
        P(None, DP, TP),
        P(None, DP, None),
        P(None, None, TP),
        P(None, None, TP),
        P(None, None, TP),
        P(None, TP),
        P(None, TP),
        P(None, TP),
        P(None, TP),
        P(None, TP, DP),
        P(None, DP, None, TP),
        P(None, DP, None, TP),
        P(None, DP, None, TP),
        P(None, DP, TP, None, None),
    )
    return jax.shard_map(
        local,
        mesh=finer,
        in_specs=placed,
        out_specs=(
            P(None, DP),
            P(None, DP, None, TP),
            P(None, DP, None, TP),
            P(None, DP, None, TP),
            P(None, DP, TP, None, None),
        ),
        check_vma=False,
    )
```

profile of v0, /device:TPU:8, one launch (start us, length us, event | category | flops | bytes accessed | tf_op | source)
XLA Modules:
  0.0 351.3 jit_solution(7885808371134442058)
XLA Ops:
  0.6 1.0 copy.87
  2.3 4.4 %all-to-all-start = ((f32[8,64,1]{1,2,0:T(1,128)}), f32[8,64,1]{1,2,0:T(1,128)S(1)}, u32[]{:S(2)}, u32[]{:S(2)}) async-start(f32[8,64,1]{1,2,0:T(1,128)} %broadcast_in_dim.24), calls=%async_computation | async-start | bytes 8192 | tf_op jit(solution)/shard_map/all_to_all | solution.py:53
  6.8 0.7 copy-done.12
  7.5 0.7 copy-done.13
  8.2 0.6 copy-done.8
  8.9 3.0 all-to-all-done
  14.3 0.6 copy-done.4
  15.3 0.7 concatenate.30
  16.0 3.4 all-to-all-start.1
  19.4 5.5 %all-to-all-done.1 = bf16[8,8,448]{2,1,0:T(8,128)(2,1)S(1)} async-done(((bf16[8,8,448]{2,1,0:T(8,128)(2,1)}), bf16[8,8,448]{2,1,0:T(8,128)(2,1)S(1)}, u32[]{:S(2)}, u32[]{:S(2)}) %all-to-all-start.1) | async-done | bytes 57376 | tf_op jit(solution)/shard_map/all_to_all | solution.py:23
  25.2 56.1 %all-gather = bf16[64,32,16]{1,2,0:T(8,128)(2,1)S(1)} all-gather(bf16[1,32,16]{1,2,0:T(8,128)(2,1)S(1)} %maximum_bitcast_fusion), channel_id=1, replica_groups=mesh['tp_0'=8,'tp_1'=8,'dp_0'=4,'dp_1'=2] {'tp_0','tp_1'}, dimensions={0}, use_global_device_ids=true | all-gather | bytes 66560 | tf_op jit(solution)/shard_map/all_gather | solution.py:37
  82.8 0.8 fusion.4
  84.0 16.0 %psum.56 = f32[8,16]{1,0:T(8,128)S(1)} all-reduce(f32[8,16]{1,0:T(8,128)S(1)} %broadcast_multiply_fusion.3), channel_id=1, replica_groups=mesh['tp_0'=8,'tp_1'=8,'dp_0'=4,'dp_1'=2] {'tp_0'}, use_global_device_ids=true, to_apply=%region_7.8 | all-reduce | flops 128 | bytes 1024 | tf_op jit(solution)/shard_map/psum | solution.py:47
  100.0 15.4 %psum.57 = f32[8,16]{1,0:T(8,128)S(1)} all-reduce(f32[8,16]{1,0:T(8,128)S(1)} %psum.56), channel_id=1, replica_groups=mesh['tp_0'=8,'tp_1'=8,'dp_0'=4,'dp_1'=2] {'tp_1'}, use_global_device_ids=true, to_apply=%region_8.9 | all-reduce | flops 128 | bytes 1024 | tf_op jit(solution)/shard_map/psum | solution.py:47
  115.6 0.6 broadcast_in_dim.28
  116.2 3.3 all-to-all-start.2
  119.7 5.1 %all-to-all-done.2 = bf16[8,8,128]{2,1,0:T(8,128)(2,1)S(1)} async-done(((bf16[8,8,128]{2,1,0:T(8,128)(2,1)}), bf16[8,8,128]{2,1,0:T(8,128)(2,1)S(1)}, u32[]{:S(2)}, u32[]{:S(2)}) %all-to-all-start.2) | async-done | bytes 16416 | tf_op jit(solution)/shard_map/all_to_all | solution.py:53
  125.2 0.8 reshape.185
  126.1 8.3 %all-to-all-start.3 = ((f32[64,1,512]{2,1,0:T(1,128)}), f32[64,1,512]{2,1,0:T(1,128)S(1)}, u32[]{:S(2)}, u32[]{:S(2)}) async-start(f32[64,1,512]{2,1,0:T(1,128)} %reshape.185), calls=%async_computation.3 | async-start | bytes 262144 | tf_op jit(solution)/shard_map/all_to_all | solution.py:71
  134.5 11.7 %all-to-all-done.3 = f32[64,1,512]{2,1,0:T(1,128)S(1)} async-done(((f32[64,1,512]{2,1,0:T(1,128)}), f32[64,1,512]{2,1,0:T(1,128)S(1)}, u32[]{:S(2)}, u32[]{:S(2)}) %all-to-all-start.3) | async-done | bytes 131104 | tf_op jit(solution)/shard_map/all_to_all | solution.py:71
  146.8 1.0 reduce.11
  148.0 14.8 %psum.58 = f32[64,1]{0,1:T(1,128)S(1)} all-reduce(f32[64,1]{0,1:T(1,128)S(1)} %bitcast.277), channel_id=1, replica_groups=mesh['tp_0'=8,'tp_1'=8,'dp_0'=4,'dp_1'=2] {'tp_0'}, use_global_device_ids=true, to_apply=%region_12.13 | all-reduce | flops 64 | bytes 512 | tf_op jit(solution)/shard_map/psum | solution.py:47
  162.8 15.4 %psum.59 = f32[64,1]{0,1:T(1,128)S(1)} all-reduce(f32[64,1]{0,1:T(1,128)S(1)} %psum.58), channel_id=1, replica_groups=mesh['tp_0'=8,'tp_1'=8,'dp_0'=4,'dp_1'=2] {'tp_1'}, use_global_device_ids=true, to_apply=%region_13.14 | all-reduce | flops 64 | bytes 512 | tf_op jit(solution)/shard_map/psum | solution.py:47
  178.2 8.9 %psum.60 = f32[64,1]{0,1:T(1,128)S(1)} all-reduce(f32[64,1]{0,1:T(1,128)S(1)} %psum.59), channel_id=1, replica_groups=mesh['tp_0'=8,'tp_1'=8,'dp_0'=4,'dp_1'=2] {'dp_0'}, use_global_device_ids=true, to_apply=%region_14.15 | all-reduce | flops 64 | bytes 512 | tf_op jit(solution)/shard_map/psum | solution.py:47
  187.1 2.5 psum.61
  189.7 0.8 reshape.187
  190.4 7.7 %all-to-all-start.4 = ((bf16[64,2,256]{2,1,0:T(2,128)(2,1)}), bf16[64,2,256]{2,1,0:T(2,128)(2,1)S(1)}, u32[]{:S(2)}, u32[]{:S(2)}) async-start(bf16[64,2,256]{2,1,0:T(2,128)(2,1)} %reshape.187), calls=%async_computation.4 | async-start | bytes 131072 | tf_op jit(solution)/shard_map/all_to_all | solution.py:53
  198.3 11.2 %all-to-all-done.4 = bf16[64,2,256]{2,1,0:T(2,128)(2,1)S(1)} async-done(((bf16[64,2,256]{2,1,0:T(2,128)(2,1)}), bf16[64,2,256]{2,1,0:T(2,128)(2,1)S(1)}, u32[]{:S(2)}, u32[]{:S(2)}) %all-to-all-start.4) | async-done | bytes 65568 | tf_op jit(solution)/shard_map/all_to_all | solution.py:53
  210.8 0.7 concatenate.35
  211.5 3.4 all-to-all-start.5
  214.9 5.5 %all-to-all-done.5 = bf16[8,8,448]{2,1,0:T(8,128)(2,1)S(1)} async-done(((bf16[8,8,448]{2,1,0:T(8,128)(2,1)}), bf16[8,8,448]{2,1,0:T(8,128)(2,1)S(1)}, u32[]{:S(2)}, u32[]{:S(2)}) %all-to-all-start.5) | async-done | bytes 57376 | tf_op jit(solution)/shard_map/all_to_all | solution.py:23
  220.8 47.6 %all-gather.1 = bf16[64,32,16]{1,2,0:T(8,128)(2,1)S(1)} all-gather(bf16[1,32,16]{1,2,0:T(8,128)(2,1)S(1)} %maximum_bitcast_fusion.1), channel_id=1, replica_groups=mesh['tp_0'=8,'tp_1'=8,'dp_0'=4,'dp_1'=2] {'tp_0','tp_1'}, dimensions={0}, use_global_device_ids=true | all-gather | bytes 66560 | tf_op jit(solution)/shard_map/all_gather | solution.py:37
  269.9 0.8 fusion.1
  271.0 14.8 %psum.62 = f32[8,16]{1,0:T(8,128)S(1)} all-reduce(f32[8,16]{1,0:T(8,128)S(1)} %broadcast_multiply_fusion.2), channel_id=1, replica_groups=mesh['tp_0'=8,'tp_1'=8,'dp_0'=4,'dp_1'=2] {'tp_0'}, use_global_device_ids=true, to_apply=%region_21.22 | all-reduce | flops 128 | bytes 1024 | tf_op jit(solution)/shard_map/psum | solution.py:47
  285.8 16.7 %psum.63 = f32[8,16]{1,0:T(8,128)S(1)} all-reduce(f32[8,16]{1,0:T(8,128)S(1)} %psum.62), channel_id=1, replica_groups=mesh['tp_0'=8,'tp_1'=8,'dp_0'=4,'dp_1'=2] {'tp_1'}, use_global_device_ids=true, to_apply=%region_22.23 | all-reduce | flops 128 | bytes 1024 | tf_op jit(solution)/shard_map/psum | solution.py:47
  302.7 0.6 broadcast_in_dim.34
  303.4 3.5 %all-to-all-start.6 = ((bf16[8,8,128]{2,1,0:T(8,128)(2,1)}), bf16[8,8,128]{2,1,0:T(8,128)(2,1)S(1)}, u32[]{:S(2)}, u32[]{:S(2)}) async-start(bf16[8,8,128]{2,1,0:T(8,128)(2,1)} %broadcast_in_dim.34), calls=%async_computation.6 | async-start | bytes 32768 | tf_op jit(solution)/shard_map/all_to_all | solution.py:53
  306.9 0.6 pad_maximum_fusion.2
  308.7 3.3 all-to-all-done.6
  312.4 0.8 reshape.189
  313.2 6.4 %all-to-all-start.7 = ((f32[64,1,512]{2,1,0:T(1,128)}), f32[64,1,512]{2,1,0:T(1,128)S(1)}, u32[]{:S(2)}, u32[]{:S(2)}) async-start(f32[64,1,512]{2,1,0:T(1,128)} %reshape.189), calls=%async_computation.7 | async-start | bytes 262144 | tf_op jit(solution)/shard_map/all_to_all | solution.py:71
  320.1 11.4 %all-to-all-done.7 = f32[64,1,512]{2,1,0:T(1,128)S(1)} async-done(((f32[64,1,512]{2,1,0:T(1,128)}), f32[64,1,512]{2,1,0:T(1,128)S(1)}, u32[]{:S(2)}, u32[]{:S(2)}) %all-to-all-start.7) | async-done | bytes 131104 | tf_op jit(solution)/shard_map/all_to_all | solution.py:71
  331.5 1.0 reduce.12
  332.7 0.8 reshape.191
  333.5 5.4 %all-to-all-start.8 = ((bf16[64,2,256]{2,1,0:T(2,128)(2,1)}), bf16[64,2,256]{2,1,0:T(2,128)(2,1)S(1)}, u32[]{:S(2)}, u32[]{:S(2)}) async-start(bf16[64,2,256]{2,1,0:T(2,128)(2,1)} %reshape.191), calls=%async_computation.8 | async-start | bytes 131072 | tf_op jit(solution)/shard_map/all_to_all | solution.py:53
  338.9 1.0 pad_maximum_fusion
  339.9 10.5 %all-to-all-done.8 = bf16[64,2,256]{2,1,0:T(2,128)(2,1)S(1)} async-done(((bf16[64,2,256]{2,1,0:T(2,128)(2,1)}), bf16[64,2,256]{2,1,0:T(2,128)(2,1)S(1)}, u32[]{:S(2)}, u32[]{:S(2)}) %all-to-all-start.8) | async-done | bytes 65568 | tf_op jit(solution)/shard_map/all_to_all | solution.py:53
  350.5 0.7 copy.102
  (145 shorter events, 13.3 us)
Async XLA Ops:
  2.3 4.4 %copy-start.14 = (f32[2,2]{1,0:T(2,128)S(1)}, f32[2,2]{1,0:T(2,128)}, u32[]{:S(2)}) copy-start(f32[2,2]{1,0:T(2,128)} %param.31) | copy-start | bytes 52
  2.3 4.5 %copy-start.10 = (f32[2,512]{1,0:T(2,128)S(1)}, f32[2,512]{1,0:T(2,128)}, u32[]{:S(2)}) copy-start(f32[2,512]{1,0:T(2,128)} %param.20) | copy-start | bytes 12292
  2.3 4.5 %copy-start.11 = (bf16[2,4,128]{2,1,0:T(4,128)(2,1)S(1)}, bf16[2,4,128]{2,1,0:T(4,128)(2,1)}, u32[]{:S(2)}) copy-start(bf16[2,4,128]{2,1,0:T(4,128)(2,1)} %param.26) | copy-start | bytes 6148
  2.3 9.6 %all-to-all-start = ((f32[8,64,1]{1,2,0:T(1,128)}), f32[8,64,1]{1,2,0:T(1,128)S(1)}, u32[]{:S(2)}, u32[]{:S(2)}) async-start(f32[8,64,1]{1,2,0:T(1,128)} %broadcast_in_dim.24), calls=%async_computation | async-start | bytes 8192 | tf_op jit(solution)/shard_map/all_to_all | solution.py:53
  6.7 1.4 copy-start.7
  6.8 0.7 copy-start.12
  7.5 0.7 copy-start.13
  8.2 0.7 copy-start.8
  8.2 0.7 copy-start.9
  8.2 0.7 copy-start.16
  8.2 0.7 copy-start.17
  8.2 0.7 copy-start.15
  8.2 3.8 %copy-start.6 = (bf16[2,512,32]{1,2,0:T(8,128)(2,1)S(1)}, bf16[2,512,32]{1,2,0:T(8,128)(2,1)}, u32[]{:S(2)}) copy-start(bf16[2,512,32]{1,2,0:T(8,128)(2,1)} %param.24) | copy-start | bytes 196612
  11.9 0.8 copy-start.5
  12.0 1.2 copy-start.3
  13.0 1.0 copy-start.2
  14.0 0.9 copy-start.4
  16.0 8.9 %all-to-all-start.1 = ((bf16[8,8,448]{2,1,0:T(8,128)(2,1)}), bf16[8,8,448]{2,1,0:T(8,128)(2,1)S(1)}, u32[]{:S(2)}, u32[]{:S(2)}) async-start(bf16[8,8,448]{2,1,0:T(8,128)(2,1)} %bitcast.6), calls=%async_computation.1 | async-start | bytes 131072 | tf_op jit(solution)/shard_map/all_to_all | solution.py:23
  81.3 1.5 copy-start
  82.8 36.8 %copy-start.1 = (bf16[2,128,512]{2,1,0:T(8,128)(2,1)S(1)}, bf16[2,128,512]{2,1,0:T(8,128)(2,1)}, u32[]{:S(2)}) copy-start(bf16[2,128,512]{2,1,0:T(8,128)(2,1)} %param.33) | copy-start | bytes 786436
  116.2 8.6 %all-to-all-start.2 = ((bf16[8,8,128]{2,1,0:T(8,128)(2,1)}), bf16[8,8,128]{2,1,0:T(8,128)(2,1)S(1)}, u32[]{:S(2)}, u32[]{:S(2)}) async-start(bf16[8,8,128]{2,1,0:T(8,128)(2,1)} %broadcast_in_dim.28), calls=%async_computation.2 | async-start | bytes 32768 | tf_op jit(solution)/shard_map/all_to_all | solution.py:53
  126.1 20.2 %all-to-all-start.3 = ((f32[64,1,512]{2,1,0:T(1,128)}), f32[64,1,512]{2,1,0:T(1,128)S(1)}, u32[]{:S(2)}, u32[]{:S(2)}) async-start(f32[64,1,512]{2,1,0:T(1,128)} %reshape.185), calls=%async_computation.3 | async-start | bytes 262144 | tf_op jit(solution)/shard_map/all_to_all | solution.py:71
  190.4 19.0 %all-to-all-start.4 = ((bf16[64,2,256]{2,1,0:T(2,128)(2,1)}), bf16[64,2,256]{2,1,0:T(2,128)(2,1)S(1)}, u32[]{:S(2)}, u32[]{:S(2)}) async-start(bf16[64,2,256]{2,1,0:T(2,128)(2,1)} %reshape.187), calls=%async_computation.4 | async-start | bytes 131072 | tf_op jit(solution)/shard_map/all_to_all | solution.py:53
  211.5 8.9 %all-to-all-start.5 = ((bf16[8,8,448]{2,1,0:T(8,128)(2,1)}), bf16[8,8,448]{2,1,0:T(8,128)(2,1)S(1)}, u32[]{:S(2)}, u32[]{:S(2)}) async-start(bf16[8,8,448]{2,1,0:T(8,128)(2,1)} %bitcast.45), calls=%async_computation.5 | async-start | bytes 131072 | tf_op jit(solution)/shard_map/all_to_all | solution.py:23
  303.4 8.6 %all-to-all-start.6 = ((bf16[8,8,128]{2,1,0:T(8,128)(2,1)}), bf16[8,8,128]{2,1,0:T(8,128)(2,1)S(1)}, u32[]{:S(2)}, u32[]{:S(2)}) async-start(bf16[8,8,128]{2,1,0:T(8,128)(2,1)} %broadcast_in_dim.34), calls=%async_computation.6 | async-start | bytes 32768 | tf_op jit(solution)/shard_map/all_to_all | solution.py:53
  313.2 18.3 %all-to-all-start.7 = ((f32[64,1,512]{2,1,0:T(1,128)}), f32[64,1,512]{2,1,0:T(1,128)S(1)}, u32[]{:S(2)}, u32[]{:S(2)}) async-start(f32[64,1,512]{2,1,0:T(1,128)} %reshape.189), calls=%async_computation.7 | async-start | bytes 262144 | tf_op jit(solution)/shard_map/all_to_all | solution.py:71
  333.5 16.9 %all-to-all-start.8 = ((bf16[64,2,256]{2,1,0:T(2,128)(2,1)}), bf16[64,2,256]{2,1,0:T(2,128)(2,1)S(1)}, u32[]{:S(2)}, u32[]{:S(2)}) async-start(bf16[64,2,256]{2,1,0:T(2,128)(2,1)} %reshape.191), calls=%async_computation.8 | async-start | bytes 131072 | tf_op jit(solution)/shard_map/all_to_all | solution.py:53
where the time goes:
time: 352 us; the launch traced here: 351 us
  blocking collectives  208 us (59%)
  waiting for transfers between devices  67.3 us (19%)
  starting transfers between devices  45.8 us (13%)
  local copies, waits for them, and re-layouts  16.8 us (5%)
  other arithmetic  7.6 us (2%)
  matrix products  4.45 us (1%)
    psum x8, blocking collectives, over_axes(): shard = lax.psum(shard, axis)  104 us
    all_gather x2, blocking collectives, gather_turned(): lax.all_gather(both, axis, axis=0, tiled=True)  104 us
    all_to_all x5, waiting for transfers between devices, copy_for_each(): lax.all_to_all(jnp.broadcast_to(shard[None], (size, *shard.shape)), axis,...  33 us
    all_to_all x5, starting transfers between devices, copy_for_each(): lax.all_to_all(jnp.broadcast_to(shard[None], (size, *shard.shape)), axis,...  24.4 us
    all_to_all x2, waiting for transfers between devices, summed_on_arrival_2(): lax.all_to_all(pieces, axis, split_axis=0, concat_axis=0, tiled=True)  23.2 us
    all_to_all x2, starting transfers between devices, summed_on_arrival_2(): lax.all_to_all(pieces, axis, split_axis=0, concat_axis=0, tiled=True)  14.7 us
    all_to_all x2, waiting for transfers between devices, summed_on_arrival(): pieces = lax.all_to_all(cut_along(shard, dim, size), axis, 0, 0, tiled=True)  11.1 us
    unnamed x52, local copies, waits for them, and re-layouts  9.87 us
  transfers between devices with their start and end apart: 9, of which 9 were waited for; matrix products, arithmetic and copies ran while one was open for 1% of the time, Pallas kernels for 0%

commit v1 on v0

--- a/solution.py
+++ b/solution.py
@@ -13,6 +13,13 @@
 eps = 1e-06
 
 
+def all_by_exchange(block, axis, d):
+    count = lax.axis_size(axis)
+    shards = jnp.stack([block for _ in range(count)])
+    shards = lax.all_to_all(shards, axis, split_axis=0, concat_axis=0)
+    return jnp.concatenate(shards, axis=d)
+
+
 def cut_along(shard, dim, size):
     before, after = (shard.shape[:dim], shard.shape[dim + 1 :])
     return jnp.moveaxis(shard.reshape(*before, size, -1, *after), dim, 0)
@@ -34,7 +41,7 @@
 def gather_turned(arrays, axis, dims):
     turned = [jnp.moveaxis(a, dim, 0) for a, dim in zip(arrays, dims)]
     both = jnp.concatenate([t.reshape(len(t), -1) for t in turned], axis=1)
-    result, at, gathered = (lax.all_gather(both, axis, axis=0, tiled=True), 0, [])
+    result, at, gathered = (all_by_exchange(both, axis, 0), 0, [])
     for t, dim in zip(turned, dims):
         share = result[:, at : at + t[0].size].reshape(-1, *t.shape[1:])
         gathered.append(jnp.moveaxis(share, 0, dim))

time: 352 us -> 293 us (0.83)
  blocking collectives: 208 us -> 102 us
  waiting for transfers between devices: 67.3 us -> 89.9 us
  starting transfers between devices: 45.8 us -> 67.9 us
    all_gather x2 -> x0, blocking collectives: 104 us -> none  [gather_turned(): lax.all_gather(both, axis, axis=0, tiled=True)]
    all_to_all x0 -> x2, starting transfers between devices: none -> 22 us  [all_by_exchange(): shards = lax.all_to_all(shards, axis, split_axis=0, concat_axis=0)]
    all_to_all x0 -> x2, waiting for transfers between devices: none -> 21.3 us  [all_by_exchange(): shards = lax.all_to_all(shards, axis, split_axis=0, concat_axis=0)]
    unnamed x52 -> x56, local copies, waits for them, and re-layouts: 9.87 us -> 11.4 us
  transfers between devices with their start and end apart: 9 -> 11, of which waited for: 9 -> 11; matrix products, arithmetic and copies ran while one was open for 1% -> 1% of each run, Pallas kernels for 0% -> 0%
where the time goes in v1:
time: 293 us; the launch traced here: 292 us
  blocking collectives  102 us (35%)
  waiting for transfers between devices  89.9 us (31%)
  starting transfers between devices  67.9 us (23%)
  local copies, waits for them, and re-layouts  18.9 us (6%)
  other arithmetic  7.6 us (3%)
  matrix products  4.45 us (2%)
    psum x8, blocking collectives, over_axes(): shard = lax.psum(shard, axis)  102 us
    all_to_all x5, waiting for transfers between devices, copy_for_each(): lax.all_to_all(jnp.broadcast_to(shard[None], (size, *shard.shape)), axis,...  34.4 us
    all_to_all x5, starting transfers between devices, copy_for_each(): lax.all_to_all(jnp.broadcast_to(shard[None], (size, *shard.shape)), axis,...  24.2 us
    all_to_all x2, waiting for transfers between devices, summed_on_arrival_2(): lax.all_to_all(pieces, axis, split_axis=0, concat_axis=0, tiled=True)  23.2 us
    all_to_all x2, starting transfers between devices, all_by_exchange(): shards = lax.all_to_all(shards, axis, split_axis=0, concat_axis=0)  22 us
    all_to_all x2, waiting for transfers between devices, all_by_exchange(): shards = lax.all_to_all(shards, axis, split_axis=0, concat_axis=0)  21.3 us
    all_to_all x2, starting transfers between devices, summed_on_arrival_2(): lax.all_to_all(pieces, axis, split_axis=0, concat_axis=0, tiled=True)  15.1 us
    unnamed x56, local copies, waits for them, and re-layouts  11.4 us
  transfers between devices with their start and end apart: 11, of which 11 were waited for; matrix products, arithmetic and copies ran while one was open for 1% of the time, Pallas kernels for 0%

profile of v1, /device:TPU:8, one launch (start us, length us, event | category | flops | bytes accessed | tf_op | source)
XLA Modules:
  0.0 292.1 jit_solution(9148775763894044777)
XLA Ops:
  0.6 1.0 copy.84
  2.3 4.4 %all-to-all-start = ((f32[8,64,1]{1,2,0:T(1,128)}), f32[8,64,1]{1,2,0:T(1,128)S(1)}, u32[]{:S(2)}, u32[]{:S(2)}) async-start(f32[8,64,1]{1,2,0:T(1,128)} %broadcast_in_dim.24), calls=%async_computation | async-start | bytes 8192 | tf_op jit(solution)/shard_map/all_to_all | solution.py:60
  6.8 0.7 copy-done.12
  7.5 0.7 copy-done.13
  8.2 0.6 copy-done.8
  8.9 3.0 %all-to-all-done = f32[8,64,1]{1,2,0:T(1,128)S(1)} async-done(((f32[8,64,1]{1,2,0:T(1,128)}), f32[8,64,1]{1,2,0:T(1,128)S(1)}, u32[]{:S(2)}, u32[]{:S(2)}) %all-to-all-start) | async-done | bytes 2080 | tf_op jit(solution)/shard_map/all_to_all | solution.py:60
  15.3 0.7 concatenate.30
  16.0 3.4 %all-to-all-start.1 = ((bf16[8,8,448]{2,1,0:T(8,128)(2,1)}), bf16[8,8,448]{2,1,0:T(8,128)(2,1)S(1)}, u32[]{:S(2)}, u32[]{:S(2)}) async-start(bf16[8,8,448]{2,1,0:T(8,128)(2,1)} %bitcast.6), calls=%async_computation.1 | async-start | bytes 131072 | tf_op jit(solution)/shard_map/all_to_all | solution.py:30
  19.4 5.5 %all-to-all-done.1 = bf16[8,8,448]{2,1,0:T(8,128)(2,1)S(1)} async-done(((bf16[8,8,448]{2,1,0:T(8,128)(2,1)}), bf16[8,8,448]{2,1,0:T(8,128)(2,1)S(1)}, u32[]{:S(2)}, u32[]{:S(2)}) %all-to-all-start.1) | async-done | bytes 57376 | tf_op jit(solution)/shard_map/all_to_all | solution.py:30
  25.3 0.8 reshape.193
  26.1 16.6 %all-to-all-start.2 = ((bf16[64,2,256]{2,1,0:T(2,128)(2,1)}), bf16[64,2,256]{2,1,0:T(2,128)(2,1)S(1)}, u32[]{:S(2)}, u32[]{:S(2)}) async-start(bf16[64,2,256]{2,1,0:T(2,128)(2,1)} %reshape.193), calls=%async_computation.2 | async-start | bytes 131072 | tf_op jit(solution)/shard_map/all_to_all | solution.py:19
  42.8 11.2 %all-to-all-done.2 = bf16[64,2,256]{2,1,0:T(2,128)(2,1)S(1)} async-done(((bf16[64,2,256]{2,1,0:T(2,128)(2,1)}), bf16[64,2,256]{2,1,0:T(2,128)(2,1)S(1)}, u32[]{:S(2)}, u32[]{:S(2)}) %all-to-all-start.2) | async-done | bytes 65568 | tf_op jit(solution)/shard_map/all_to_all | solution.py:19
  55.6 0.8 fusion.4
  56.8 14.8 %psum.56 = f32[8,16]{1,0:T(8,128)S(1)} all-reduce(f32[8,16]{1,0:T(8,128)S(1)} %broadcast_multiply_fusion.3), channel_id=1, replica_groups=mesh['tp_0'=8,'tp_1'=8,'dp_0'=4,'dp_1'=2] {'tp_0'}, use_global_device_ids=true, to_apply=%region_7.8 | all-reduce | flops 128 | bytes 1024 | tf_op jit(solution)/shard_map/psum | solution.py:54
  71.5 15.4 %psum.57 = f32[8,16]{1,0:T(8,128)S(1)} all-reduce(f32[8,16]{1,0:T(8,128)S(1)} %psum.56), channel_id=1, replica_groups=mesh['tp_0'=8,'tp_1'=8,'dp_0'=4,'dp_1'=2] {'tp_1'}, use_global_device_ids=true, to_apply=%region_8.9 | all-reduce | flops 128 | bytes 1024 | tf_op jit(solution)/shard_map/psum | solution.py:54
  87.8 3.3 %all-to-all-start.3 = ((bf16[8,8,128]{2,1,0:T(8,128)(2,1)}), bf16[8,8,128]{2,1,0:T(8,128)(2,1)S(1)}, u32[]{:S(2)}, u32[]{:S(2)}) async-start(bf16[8,8,128]{2,1,0:T(8,128)(2,1)} %broadcast_in_dim.28), calls=%async_computation.3 | async-start | bytes 32768 | tf_op jit(solution)/shard_map/all_to_all | solution.py:60
  91.3 5.1 %all-to-all-done.3 = bf16[8,8,128]{2,1,0:T(8,128)(2,1)S(1)} async-done(((bf16[8,8,128]{2,1,0:T(8,128)(2,1)}), bf16[8,8,128]{2,1,0:T(8,128)(2,1)S(1)}, u32[]{:S(2)}, u32[]{:S(2)}) %all-to-all-start.3) | async-done | bytes 16416 | tf_op jit(solution)/shard_map/all_to_all | solution.py:60
  96.8 0.8 reshape.195
  97.7 7.5 %all-to-all-start.4 = ((f32[64,1,512]{2,1,0:T(1,128)}), f32[64,1,512]{2,1,0:T(1,128)S(1)}, u32[]{:S(2)}, u32[]{:S(2)}) async-start(f32[64,1,512]{2,1,0:T(1,128)} %reshape.195), calls=%async_computation.4 | async-start | bytes 262144 | tf_op jit(solution)/shard_map/all_to_all | solution.py:78
  105.3 11.7 %all-to-all-done.4 = f32[64,1,512]{2,1,0:T(1,128)S(1)} async-done(((f32[64,1,512]{2,1,0:T(1,128)}), f32[64,1,512]{2,1,0:T(1,128)S(1)}, u32[]{:S(2)}, u32[]{:S(2)}) %all-to-all-start.4) | async-done | bytes 131104 | tf_op jit(solution)/shard_map/all_to_all | solution.py:78
  117.6 1.0 reduce.11
  118.8 14.8 %psum.58 = f32[64,1]{0,1:T(1,128)S(1)} all-reduce(f32[64,1]{0,1:T(1,128)S(1)} %bitcast.281), channel_id=1, replica_groups=mesh['tp_0'=8,'tp_1'=8,'dp_0'=4,'dp_1'=2] {'tp_0'}, use_global_device_ids=true, to_apply=%region_12.13 | all-reduce | flops 64 | bytes 512 | tf_op jit(solution)/shard_map/psum | solution.py:54
  133.6 15.4 %psum.59 = f32[64,1]{0,1:T(1,128)S(1)} all-reduce(f32[64,1]{0,1:T(1,128)S(1)} %psum.58), channel_id=1, replica_groups=mesh['tp_0'=8,'tp_1'=8,'dp_0'=4,'dp_1'=2] {'tp_1'}, use_global_device_ids=true, to_apply=%region_13.14 | all-reduce | flops 64 | bytes 512 | tf_op jit(solution)/shard_map/psum | solution.py:54
  149.0 8.9 %psum.60 = f32[64,1]{0,1:T(1,128)S(1)} all-reduce(f32[64,1]{0,1:T(1,128)S(1)} %psum.59), channel_id=1, replica_groups=mesh['tp_0'=8,'tp_1'=8,'dp_0'=4,'dp_1'=2] {'dp_0'}, use_global_device_ids=true, to_apply=%region_14.15 | all-reduce | flops 64 | bytes 512 | tf_op jit(solution)/shard_map/psum | solution.py:54
  157.9 2.5 psum.61
  160.5 0.8 reshape.197
  161.3 7.7 %all-to-all-start.5 = ((bf16[64,2,256]{2,1,0:T(2,128)(2,1)}), bf16[64,2,256]{2,1,0:T(2,128)(2,1)S(1)}, u32[]{:S(2)}, u32[]{:S(2)}) async-start(bf16[64,2,256]{2,1,0:T(2,128)(2,1)} %reshape.197), calls=%async_computation.5 | async-start | bytes 131072 | tf_op jit(solution)/shard_map/all_to_all | solution.py:60
  169.1 11.2 %all-to-all-done.5 = bf16[64,2,256]{2,1,0:T(2,128)(2,1)S(1)} async-done(((bf16[64,2,256]{2,1,0:T(2,128)(2,1)}), bf16[64,2,256]{2,1,0:T(2,128)(2,1)S(1)}, u32[]{:S(2)}, u32[]{:S(2)}) %all-to-all-start.5) | async-done | bytes 65568 | tf_op jit(solution)/shard_map/all_to_all | solution.py:60
  181.6 0.7 concatenate.35
  182.3 3.4 %all-to-all-start.6 = ((bf16[8,8,448]{2,1,0:T(8,128)(2,1)}), bf16[8,8,448]{2,1,0:T(8,128)(2,1)S(1)}, u32[]{:S(2)}, u32[]{:S(2)}) async-start(bf16[8,8,448]{2,1,0:T(8,128)(2,1)} %bitcast.44), calls=%async_computation.6 | async-start | bytes 131072 | tf_op jit(solution)/shard_map/all_to_all | solution.py:30
  185.7 5.5 %all-to-all-done.6 = bf16[8,8,448]{2,1,0:T(8,128)(2,1)S(1)} async-done(((bf16[8,8,448]{2,1,0:T(8,128)(2,1)}), bf16[8,8,448]{2,1,0:T(8,128)(2,1)S(1)}, u32[]{:S(2)}, u32[]{:S(2)}) %all-to-all-start.6) | async-done | bytes 57376 | tf_op jit(solution)/shard_map/all_to_all | solution.py:30
  191.6 0.8 reshape.199
  192.4 5.4 %all-to-all-start.7 = ((bf16[64,2,256]{2,1,0:T(2,128)(2,1)}), bf16[64,2,256]{2,1,0:T(2,128)(2,1)S(1)}, u32[]{:S(2)}, u32[]{:S(2)}) async-start(bf16[64,2,256]{2,1,0:T(2,128)(2,1)} %reshape.199), calls=%async_computation.7 | async-start | bytes 131072 | tf_op jit(solution)/shard_map/all_to_all | solution.py:19
  199.2 10.0 %all-to-all-done.7 = bf16[64,2,256]{2,1,0:T(2,128)(2,1)S(1)} async-done(((bf16[64,2,256]{2,1,0:T(2,128)(2,1)}), bf16[64,2,256]{2,1,0:T(2,128)(2,1)S(1)}, u32[]{:S(2)}, u32[]{:S(2)}) %all-to-all-start.7) | async-done | bytes 65568 | tf_op jit(solution)/shard_map/all_to_all | solution.py:19
  210.8 0.8 fusion.1
  212.0 14.8 %psum.62 = f32[8,16]{1,0:T(8,128)S(1)} all-reduce(f32[8,16]{1,0:T(8,128)S(1)} %broadcast_multiply_fusion.2), channel_id=1, replica_groups=mesh['tp_0'=8,'tp_1'=8,'dp_0'=4,'dp_1'=2] {'tp_0'}, use_global_device_ids=true, to_apply=%region_21.22 | all-reduce | flops 128 | bytes 1024 | tf_op jit(solution)/shard_map/psum | solution.py:54
  226.7 15.5 %psum.63 = f32[8,16]{1,0:T(8,128)S(1)} all-reduce(f32[8,16]{1,0:T(8,128)S(1)} %psum.62), channel_id=1, replica_groups=mesh['tp_0'=8,'tp_1'=8,'dp_0'=4,'dp_1'=2] {'tp_1'}, use_global_device_ids=true, to_apply=%region_22.23 | all-reduce | flops 128 | bytes 1024 | tf_op jit(solution)/shard_map/psum | solution.py:54
  243.1 3.3 %all-to-all-start.8 = ((bf16[8,8,128]{2,1,0:T(8,128)(2,1)}), bf16[8,8,128]{2,1,0:T(8,128)(2,1)S(1)}, u32[]{:S(2)}, u32[]{:S(2)}) async-start(bf16[8,8,128]{2,1,0:T(8,128)(2,1)} %broadcast_in_dim.34), calls=%async_computation.8 | async-start | bytes 32768 | tf_op jit(solution)/shard_map/all_to_all | solution.py:60
  247.0 4.7 %all-to-all-done.8 = bf16[8,8,128]{2,1,0:T(8,128)(2,1)S(1)} async-done(((bf16[8,8,128]{2,1,0:T(8,128)(2,1)}), bf16[8,8,128]{2,1,0:T(8,128)(2,1)S(1)}, u32[]{:S(2)}, u32[]{:S(2)}) %all-to-all-start.8) | async-done | bytes 16416 | tf_op jit(solution)/shard_map/all_to_all | solution.py:60
  252.1 0.8 reshape.201
  252.9 7.5 %all-to-all-start.9 = ((f32[64,1,512]{2,1,0:T(1,128)}), f32[64,1,512]{2,1,0:T(1,128)S(1)}, u32[]{:S(2)}, u32[]{:S(2)}) async-start(f32[64,1,512]{2,1,0:T(1,128)} %reshape.201), calls=%async_computation.9 | async-start | bytes 262144 | tf_op jit(solution)/shard_map/all_to_all | solution.py:78
  260.9 11.4 %all-to-all-done.9 = f32[64,1,512]{2,1,0:T(1,128)S(1)} async-done(((f32[64,1,512]{2,1,0:T(1,128)}), f32[64,1,512]{2,1,0:T(1,128)S(1)}, u32[]{:S(2)}, u32[]{:S(2)}) %all-to-all-start.9) | async-done | bytes 131104 | tf_op jit(solution)/shard_map/all_to_all | solution.py:78
  272.3 1.0 reduce.12
  273.5 0.8 reshape.203
  274.3 5.4 %all-to-all-start.10 = ((bf16[64,2,256]{2,1,0:T(2,128)(2,1)}), bf16[64,2,256]{2,1,0:T(2,128)(2,1)S(1)}, u32[]{:S(2)}, u32[]{:S(2)}) async-start(bf16[64,2,256]{2,1,0:T(2,128)(2,1)} %reshape.203), calls=%async_computation.10 | async-start | bytes 131072 | tf_op jit(solution)/shard_map/all_to_all | solution.py:60
  279.7 1.0 pad_maximum_fusion
  280.7 10.5 %all-to-all-done.10 = bf16[64,2,256]{2,1,0:T(2,128)(2,1)S(1)} async-done(((bf16[64,2,256]{2,1,0:T(2,128)(2,1)}), bf16[64,2,256]{2,1,0:T(2,128)(2,1)S(1)}, u32[]{:S(2)}, u32[]{:S(2)}) %all-to-all-start.10) | async-done | bytes 65568 | tf_op jit(solution)/shard_map/all_to_all | solution.py:60
  291.3 0.7 copy.99
  (153 shorter events, 16.3 us)
Async XLA Ops:
  2.3 4.4 %copy-start.14 = (f32[2,2]{1,0:T(2,128)S(1)}, f32[2,2]{1,0:T(2,128)}, u32[]{:S(2)}) copy-start(f32[2,2]{1,0:T(2,128)} %param.31) | copy-start | bytes 52
  2.3 4.5 %copy-start.10 = (f32[2,512]{1,0:T(2,128)S(1)}, f32[2,512]{1,0:T(2,128)}, u32[]{:S(2)}) copy-start(f32[2,512]{1,0:T(2,128)} %param.20) | copy-start | bytes 12292
  2.3 4.5 %copy-start.11 = (bf16[2,4,128]{2,1,0:T(4,128)(2,1)S(1)}, bf16[2,4,128]{2,1,0:T(4,128)(2,1)}, u32[]{:S(2)}) copy-start(bf16[2,4,128]{2,1,0:T(4,128)(2,1)} %param.26) | copy-start | bytes 6148
  2.3 9.6 %all-to-all-start = ((f32[8,64,1]{1,2,0:T(1,128)}), f32[8,64,1]{1,2,0:T(1,128)S(1)}, u32[]{:S(2)}, u32[]{:S(2)}) async-start(f32[8,64,1]{1,2,0:T(1,128)} %broadcast_in_dim.24), calls=%async_computation | async-start | bytes 8192 | tf_op jit(solution)/shard_map/all_to_all | solution.py:60
  6.7 1.4 copy-start.7
  6.8 0.7 copy-start.12
  7.5 0.7 copy-start.13
  8.2 0.7 copy-start.8
  8.2 0.7 copy-start.9
  8.2 0.7 copy-start.16
  8.2 0.7 copy-start.17
  8.2 0.7 copy-start.15
  8.2 3.8 %copy-start.6 = (bf16[2,512,32]{1,2,0:T(8,128)(2,1)S(1)}, bf16[2,512,32]{1,2,0:T(8,128)(2,1)}, u32[]{:S(2)}) copy-start(bf16[2,512,32]{1,2,0:T(8,128)(2,1)} %param.24) | copy-start | bytes 196612
  11.9 0.8 copy-start.5
  12.0 1.2 copy-start.3
  13.0 1.0 copy-start.2
  14.0 0.9 copy-start.4
  16.0 8.9 %all-to-all-start.1 = ((bf16[8,8,448]{2,1,0:T(8,128)(2,1)}), bf16[8,8,448]{2,1,0:T(8,128)(2,1)S(1)}, u32[]{:S(2)}, u32[]{:S(2)}) async-start(bf16[8,8,448]{2,1,0:T(8,128)(2,1)} %bitcast.6), calls=%async_computation.1 | async-start | bytes 131072 | tf_op jit(solution)/shard_map/all_to_all | solution.py:30
  26.1 28.0 %all-to-all-start.2 = ((bf16[64,2,256]{2,1,0:T(2,128)(2,1)}), bf16[64,2,256]{2,1,0:T(2,128)(2,1)S(1)}, u32[]{:S(2)}, u32[]{:S(2)}) async-start(bf16[64,2,256]{2,1,0:T(2,128)(2,1)} %reshape.193), calls=%async_computation.2 | async-start | bytes 131072 | tf_op jit(solution)/shard_map/all_to_all | solution.py:19
  54.2 1.4 copy-start
  55.6 35.5 %copy-start.1 = (bf16[2,128,512]{2,1,0:T(8,128)(2,1)S(1)}, bf16[2,128,512]{2,1,0:T(8,128)(2,1)}, u32[]{:S(2)}) copy-start(bf16[2,128,512]{2,1,0:T(8,128)(2,1)} %param.33) | copy-start | bytes 786436
  87.8 8.6 %all-to-all-start.3 = ((bf16[8,8,128]{2,1,0:T(8,128)(2,1)}), bf16[8,8,128]{2,1,0:T(8,128)(2,1)S(1)}, u32[]{:S(2)}, u32[]{:S(2)}) async-start(bf16[8,8,128]{2,1,0:T(8,128)(2,1)} %broadcast_in_dim.28), calls=%async_computation.3 | async-start | bytes 32768 | tf_op jit(solution)/shard_map/all_to_all | solution.py:60
  97.7 19.4 %all-to-all-start.4 = ((f32[64,1,512]{2,1,0:T(1,128)}), f32[64,1,512]{2,1,0:T(1,128)S(1)}, u32[]{:S(2)}, u32[]{:S(2)}) async-start(f32[64,1,512]{2,1,0:T(1,128)} %reshape.195), calls=%async_computation.4 | async-start | bytes 262144 | tf_op jit(solution)/shard_map/all_to_all | solution.py:78
  161.3 19.0 %all-to-all-start.5 = ((bf16[64,2,256]{2,1,0:T(2,128)(2,1)}), bf16[64,2,256]{2,1,0:T(2,128)(2,1)S(1)}, u32[]{:S(2)}, u32[]{:S(2)}) async-start(bf16[64,2,256]{2,1,0:T(2,128)(2,1)} %reshape.197), calls=%async_computation.5 | async-start | bytes 131072 | tf_op jit(solution)/shard_map/all_to_all | solution.py:60
  182.3 8.9 %all-to-all-start.6 = ((bf16[8,8,448]{2,1,0:T(8,128)(2,1)}), bf16[8,8,448]{2,1,0:T(8,128)(2,1)S(1)}, u32[]{:S(2)}, u32[]{:S(2)}) async-start(bf16[8,8,448]{2,1,0:T(8,128)(2,1)} %bitcast.44), calls=%async_computation.6 | async-start | bytes 131072 | tf_op jit(solution)/shard_map/all_to_all | solution.py:30
  192.4 16.9 %all-to-all-start.7 = ((bf16[64,2,256]{2,1,0:T(2,128)(2,1)}), bf16[64,2,256]{2,1,0:T(2,128)(2,1)S(1)}, u32[]{:S(2)}, u32[]{:S(2)}) async-start(bf16[64,2,256]{2,1,0:T(2,128)(2,1)} %reshape.199), calls=%async_computation.7 | async-start | bytes 131072 | tf_op jit(solution)/shard_map/all_to_all | solution.py:19
  243.1 8.6 %all-to-all-start.8 = ((bf16[8,8,128]{2,1,0:T(8,128)(2,1)}), bf16[8,8,128]{2,1,0:T(8,128)(2,1)S(1)}, u32[]{:S(2)}, u32[]{:S(2)}) async-start(bf16[8,8,128]{2,1,0:T(8,128)(2,1)} %broadcast_in_dim.34), calls=%async_computation.8 | async-start | bytes 32768 | tf_op jit(solution)/shard_map/all_to_all | solution.py:60
  252.9 19.4 %all-to-all-start.9 = ((f32[64,1,512]{2,1,0:T(1,128)}), f32[64,1,512]{2,1,0:T(1,128)S(1)}, u32[]{:S(2)}, u32[]{:S(2)}) async-start(f32[64,1,512]{2,1,0:T(1,128)} %reshape.201), calls=%async_computation.9 | async-start | bytes 262144 | tf_op jit(solution)/shard_map/all_to_all | solution.py:78
  274.3 16.9 %all-to-all-start.10 = ((bf16[64,2,256]{2,1,0:T(2,128)(2,1)}), bf16[64,2,256]{2,1,0:T(2,128)(2,1)S(1)}, u32[]{:S(2)}, u32[]{:S(2)}) async-start(bf16[64,2,256]{2,1,0:T(2,128)(2,1)} %reshape.203), calls=%async_computation.10 | async-start | bytes 131072 | tf_op jit(solution)/shard_map/all_to_all | solution.py:60
